TPU v7x, 32 devices: a whole 2x2x4 slice. The times are simulated.
32 devices in a mesh: sp: 8 (over z, x), tp: 4 (over y, core).
Axes of the slice: x: 2, y: 2, z: 4, core: 2. Of those that a mesh axis runs over, the one named last changes fastest.
Arguments:
- residual_in: bfloat16 [1536, 2048], P('sp', 'tp'), may hold values from -6 to 6
- query_rows: bfloat16 [1536, 1024], P('sp', 'tp'), may hold values from -8 to 8
- key_rows: bfloat16 [1536, 1024], P('sp', 'tp'), may hold values from -8 to 8
- value_rows: bfloat16 [1536, 1024], P('sp', 'tp'), may hold values from -6 to 6
- map_weight: float32 [16], P('tp'), may hold values from 0.3 to 0.8
- head_gain: float32 [64], replicated, may hold values from 0.1 to 1.9
- out_proj: bfloat16 [1024, 2048], P(None, 'tp'), may hold values from -0.1875 to 0.1875
- norm_gain: float32 [2048], replicated, may hold values from 0.1 to 1.9
- route_ids: int32 [1536, 2], P('sp'), may hold values from 0 to 7, all different within a row; in each aligned block of 192 rows (0 to 191, 192 to 383, ...) at most 60 rows name the same one
- route_weights: float32 [1536, 2], P('sp'), may hold values from 0.2 to 1.2
- expert_gate: bfloat16 [8, 1024, 2048], P('sp', 'tp'), may hold values from -0.125 to 0.125
- expert_up: bfloat16 [8, 1024, 2048], P('sp', 'tp'), may hold values from -0.125 to 0.125
- expert_down: bfloat16 [8, 1024, 2048], P('sp', None, 'tp'), may hold values from -0.1875 to 0.1875
- shared_gate: bfloat16 [1024, 2048], P('tp'), may hold values from -0.125 to 0.125
- shared_up: bfloat16 [1024, 2048], P('tp'), may hold values from -0.125 to 0.125
- shared_down: bfloat16 [1024, 2048], P(None, 'tp'), may hold values from -0.1875 to 0.1875
Outputs:
- mixed_out: bfloat16 [1536, 2048], P('sp', 'tp')
Inputs may be any that keep to these rules, and one draw needn't show every extreme that they name: `route_ids`: each row names 2 different experts. Among the rows held by one index of sp no expert is named more than 60 times, and in every draw some expert is named exactly 60 times by the rows of some index of sp.
All inputs are finite; a program needn't handle non-finite values.
Results may differ from a plain program's by a relative error of at most 0.0095.
Values may be sent and summed in bfloat16 or wider, within the bound.
A program may use at most 64 MiB of HBM per device.

v0:
```python
import jax
import jax.numpy as jnp
from jax import lax
from jax.sharding import PartitionSpec as P

epsilon = 1e-06
masked_score = -1e30


def rms_scale(values, gain_vec):
    squares = jnp.mean(values * values, axis=-1, keepdims=True)
    return values * lax.rsqrt(squares + epsilon) * gain_vec


def block_slots(route_block, experts_all, capacity):
    flat_ids = route_block.reshape(-1)
    one_hot = (flat_ids[:, None] == jnp.arange(experts_all, dtype=jnp.int32)[None, :]).astype(
        jnp.int32
    )
    earlier = jnp.cumsum(one_hot, axis=0) - one_hot
    position = jnp.sum(earlier * one_hot, axis=1)
    return (flat_ids * capacity + position).reshape(route_block.shape)


def body(
    residual_in,
    query_rows,
    key_rows,
    value_rows,
    map_weight,
    head_gain,
    out_proj,
    norm_gain,
    route_ids,
    route_weights,
    expert_gate,
    expert_up,
    expert_down,
    shared_gate,
    shared_up,
    shared_down,
):
    seq_dev = residual_in.shape[0]
    col_dev = residual_in.shape[1]
    heads_here = map_weight.shape[0]
    head_dim = head_gain.shape[0]
    half_dim = head_dim // 2
    topk_count = route_ids.shape[1]
    exp_here = expert_gate.shape[0]
    experts_all = exp_here * lax.axis_size("sp")
    capacity = 5 * seq_dev * topk_count // (4 * experts_all)
    score_scale = half_dim ** (-0.5)
    query_pos = lax.axis_index("sp") * seq_dev + jnp.arange(seq_dev, dtype=jnp.int32)
    query_heads = query_rows.reshape(seq_dev, heads_here, 2, half_dim)
    key_piece = lax.all_gather(key_rows, "sp", axis=0, tiled=True)
    value_piece = lax.all_gather(value_rows, "sp", axis=0, tiled=True)
    piece_len = key_piece.shape[0]
    key_heads = key_piece.reshape(piece_len, heads_here, 2, half_dim)
    value_heads = value_piece.reshape(piece_len, heads_here, head_dim)
    scores = (
        jnp.einsum("qhmd,khmd->mhqk", query_heads, key_heads, preferred_element_type=jnp.float32)
        * score_scale
    )
    key_pos = jnp.arange(piece_len, dtype=jnp.int32)
    visible = key_pos[None, :] <= query_pos[:, None]
    scores = jnp.where(visible, scores, masked_score)
    run_max = jnp.full((2, heads_here, seq_dev), masked_score, jnp.float32)
    new_max = jnp.maximum(run_max, jnp.max(scores, axis=-1))
    expo = jnp.where(visible, jnp.exp(scores - new_max[..., None]), 0.0)
    new_sum = jnp.sum(expo, axis=-1)
    product = jnp.einsum(
        "mhqk,khd->mhqd", expo.astype(jnp.bfloat16), value_heads, preferred_element_type=jnp.float32
    )
    summed = product / new_sum[..., None]
    diff_out = summed[0] - map_weight[:, None, None] * summed[1]
    head_out = rms_scale(diff_out, head_gain).astype(jnp.bfloat16)
    head_out = jnp.transpose(head_out, (1, 0, 2)).reshape(seq_dev, heads_here * head_dim)
    attn = jnp.dot(
        lax.all_gather(head_out, "tp", axis=1, tiled=True),
        out_proj,
        preferred_element_type=jnp.float32,
    )
    hidden_state = (residual_in.astype(jnp.float32) + attn).astype(jnp.bfloat16)
    full_rows = lax.all_gather(hidden_state, "tp", axis=1, tiled=True)
    normed = rms_scale(full_rows.astype(jnp.float32), norm_gain).astype(jnp.bfloat16)
    shared_gate_part = jnp.einsum(
        "rd,fd->rf", normed, shared_gate, preferred_element_type=jnp.float32
    )
    shared_up_part = jnp.einsum("rd,fd->rf", normed, shared_up, preferred_element_type=jnp.float32)
    shared_hidden = (jax.nn.silu(shared_gate_part) * shared_up_part).astype(jnp.bfloat16)
    slot_ids = block_slots(route_ids, experts_all, capacity)
    token_of = jnp.repeat(jnp.arange(seq_dev, dtype=jnp.int32), topk_count)
    slot_token = (
        jnp.full((experts_all * capacity,), seq_dev, jnp.int32)
        .at[slot_ids.reshape(-1)]
        .set(token_of)
    )
    own_cols = lax.dynamic_slice_in_dim(normed, lax.axis_index("tp") * col_dev, col_dev, 1)
    padded = jnp.concatenate([own_cols, jnp.zeros((1, col_dev), jnp.bfloat16)], axis=0)
    outgoing = jnp.take(padded, slot_token, axis=0).reshape(experts_all, capacity, col_dev)
    arrived = lax.all_to_all(outgoing, "sp", split_axis=0, concat_axis=1, tiled=True)
    arrived_rows = arrived.shape[1]
    pieces = lax.all_gather(arrived, "tp", axis=2, tiled=True)
    gate_add = jnp.einsum("erd,efd->erf", pieces, expert_gate, preferred_element_type=jnp.float32)
    up_add = jnp.einsum("erd,efd->erf", pieces, expert_up, preferred_element_type=jnp.float32)
    expert_hidden = (jax.nn.silu(gate_add) * up_add).astype(jnp.bfloat16)
    expert_flat = expert_hidden.reshape(exp_here * arrived_rows, expert_hidden.shape[2])
    pieces = (
        lax.all_gather(shared_hidden, "tp", axis=1, tiled=True),
        lax.all_gather(expert_flat, "tp", axis=1, tiled=True),
    )
    piece_width = pieces[0].shape[1]
    routed_piece = pieces[1].reshape(exp_here, arrived_rows, piece_width)
    shared_add = jnp.dot(pieces[0], shared_down, preferred_element_type=jnp.float32)
    expert_add = jnp.einsum(
        "erf,efd->erd", routed_piece, expert_down, preferred_element_type=jnp.float32
    )
    returned_rows = lax.all_to_all(
        expert_add.astype(jnp.bfloat16), "sp", split_axis=1, concat_axis=0, tiled=True
    )
    returned_flat = returned_rows.reshape(experts_all * capacity, col_dev)
    picked = (
        jnp.take(returned_flat, slot_ids.reshape(-1), axis=0)
        .reshape(seq_dev, topk_count, col_dev)
        .astype(jnp.float32)
    )
    routed = jnp.sum(picked * route_weights[:, :, None], axis=1)
    return (hidden_state.astype(jnp.float32) + shared_add + routed).astype(jnp.bfloat16)


def solution(mesh):
    in_specs = (
        P("sp", "tp"),
        P("sp", "tp"),
        P("sp", "tp"),
        P("sp", "tp"),
        P("tp"),
        P(),
        P(None, "tp"),
        P(),
        P("sp", None),
        P("sp", None),
        P("sp", "tp", None),
        P("sp", "tp", None),
        P("sp", None, "tp"),
        P("tp", None),
        P("tp", None),
        P(None, "tp"),
    )
    out_specs = P("sp", "tp")
    return jax.shard_map(body, mesh=mesh, in_specs=in_specs, out_specs=out_specs, check_vma=False)
```

profile of v0, /device:TPU:0, one launch (start us, length us, event | category | flops | bytes accessed | tf_op | source)
XLA Modules:
  0.0 206.6 jit_solution(2744693201549045714)
XLA Ops:
  6.5 0.9 copy.68
  7.4 0.1 eq.26
  7.6 0.1 reshape.160
  7.7 0.7 broadcast_multiply_fusion
  8.4 0.8 reduce-window.6
  9.3 0.2 slice_reduce_fusion
  9.6 0.1 mul.124
  9.8 0.1 reshape.188
  10.1 2.9 %scatter_custom_fusion = s32[480]{0:T(512)S(1)} fusion(s32[384]{0:T(512)S(1)} %fusion.40, s32[384]{0:T(512)S(1)} %reshape.188, s32[]{:T(128)} %constant.26.clone.1), kind=kCustom, calls=%fused_computation.66 | custom fusion | bytes 1924 | tf_op jit(solution)/shard_map/scatter | solution.py:96
  13.0 0.2 iota_compare_fusion
  13.3 34.1 %all_gather.21 = bf16[1536,256]{1,0:T(8,128)(2,1)S(1)} all-gather(bf16[192,256]{1,0:T(8,128)(2,1)} %param.18), channel_id=1, replica_groups=mesh['sp'=8,'tp'=4] {'sp'}, dimensions={0}, use_global_device_ids=true | all-gather | bytes 884736 | tf_op jit(solution)/shard_map/all_gather | solution.py:55
  47.4 0.3 copy.61
  47.6 1.0 copy.60
  48.6 1.9 fusion
  50.5 4.4 %fusion.1 = (f32[2,4,192]{2,1,0:T(4,128)S(1)}, bf16[2,4,192,1536]{3,2,1,0:T(8,128)(2,1)}) fusion(f32[2,4,192,1536]{3,2,1,0:T(8,128)S(1)} %get-tuple-element.8, f32[2,4,192]{2,1,0:T(4,128)S(1)} %broadcast_maximum_fusion, pred[192,1536]{1,0:T(8,128)(4,1)S(1)} %iota_compare_fusion), kind=kLoop, calls=%fused_computation.6 | loop fusion | flops 14154240 | bytes 14462976 | tf_op jit(solution)/shard_map/reduce_sum | solution.py:70
  55.0 32.1 %all_gather.22 = bf16[1536,256]{1,0:T(8,128)(2,1)S(1)} all-gather(bf16[192,256]{1,0:T(8,128)(2,1)S(1)} %copy-done.2), channel_id=1, replica_groups=mesh['sp'=8,'tp'=4] {'sp'}, dimensions={0}, use_global_device_ids=true | all-gather | bytes 884736 | tf_op jit(solution)/shard_map/all_gather | solution.py:56
  87.1 0.3 copy.64
  87.4 4.0 %fusion.29 = f32[2,4,192,64]{2,3,0,1:T(8,128)S(1)} fusion(bf16[1536,4,64,1]{0,2,3,1:T(8,128)(2,1)S(1)} %bitcast.84, bf16[2,4,192,1536]{3,2,1,0:T(8,128)(2,1)} %get-tuple-element.6, f32[2,4,192]{2,0,1:T(2,128)S(1)} %copy.66), kind=kOutput, calls=%fused_computation.35 | convolution fusion | flops 302088192 | bytes 5904384 | tf_op jit(solution)/shard_map/mhqk,khd->mhqd/dot_general | solution.py:71
  91.7 7.2 %all_gather.23 = bf16[192,1024]{0,1:T(8,128)(2,1)S(1)} all-gather(bf16[192,256]{0,1:T(8,128)(2,1)S(1)} %bitcast.85), channel_id=1, replica_groups=mesh['sp'=8,'tp'=4] {'tp'}, dimensions={1}, use_global_device_ids=true | all-gather | bytes 491520 | tf_op jit(solution)/shard_map/all_gather | solution.py:79
  98.9 1.1 fusion.23
  100.0 8.9 %all_gather.24 = bf16[192,2048]{1,0:T(8,128)(2,1)S(1)} all-gather(bf16[192,512]{1,0:T(8,128)(2,1)} %fusion.23), channel_id=1, replica_groups=mesh['sp'=8,'tp'=4] {'tp'}, dimensions={1}, use_global_device_ids=true | all-gather | bytes 983040 | tf_op jit(solution)/shard_map/all_gather | solution.py:84
  108.9 0.2 fusion.9
  109.2 0.3 fusion.11
  109.5 2.1 %gather_fusion = bf16[480,512]{1,0:T(8,128)(2,1)S(1)} fusion(bf16[193,512]{1,0:T(8,128)(2,1)S(1)} %concatenate.3, s32[1024]{0:T(1024)S(1)} %pad_clamp_fusion.1), kind=kCustom, calls=%fused_computation | custom fusion | bytes 984960 | tf_op jit(solution)/shard_map/jit(_take)/gather | solution.py:100
  111.8 0.1 broadcast_select_fusion.1
  112.0 20.3 %all_to_all.21 = bf16[8,60,512]{2,1,0:T(8,128)(2,1)S(1)} all-to-all(bf16[8,60,512]{2,1,0:T(8,128)(2,1)S(1)} %broadcast_select_fusion.1), channel_id=1, replica_groups=mesh['sp'=8,'tp'=4] {'sp'}, dimensions={0} | all-to-all | bytes 983040 | tf_op jit(solution)/shard_map/all_to_all | solution.py:101
  132.3 0.9 all_to_all.7
  133.2 0.1 reduce_sum.53
  133.4 20.1 %all-gather.2.cloned.1.call-done = bf16[1,480,2048]{2,1,0:T(8,128)(2,1)} async-done(((bf16[1,480,512]{2,1,0:T(8,128)(2,1)}), bf16[1,480,2048]{2,1,0:T(8,128)(2,1)}) %all-gather.2.cloned.1.call-update) | async-done | bytes 1966096 | tf_op jit(solution)/shard_map/all_gather | solution.py:103
  153.6 2.7 %fusion.7 = f32[480,256]{1,0:T(8,128)S(1)} fusion(bf16[1,480,2048]{2,1,0:T(8,128)(2,1)} %all-gather.2.cloned.1.call-done, bf16[1,256,2048]{2,1,0:T(8,128)(2,1)} %param.26), kind=kOutput, calls=%fused_computation.12 | convolution fusion | flops 503316480 | bytes 3506176 | tf_op jit(solution)/shard_map/erd,efd->erf/dot_general | solution.py:104
  156.3 0.7 fusion.20
  157.0 9.8 %all_gather.27 = bf16[480,1024]{1,0:T(8,128)(2,1)S(1)} all-gather(bf16[480,256]{1,0:T(8,128)(2,1)S(1)} %fusion.20), channel_id=1, replica_groups=mesh['sp'=8,'tp'=4] {'tp'}, dimensions={1}, use_global_device_ids=true | all-gather | bytes 1228800 | tf_op jit(solution)/shard_map/all_gather | solution.py:110
  166.8 0.7 fusion.15
  167.5 0.8 copy.95
  168.3 0.6 broadcast.119
  168.9 3.7 %reduce.4 = bf16[480,512]{1,0:T(8,128)(2,1)S(1)} reduce(bf16[480,1,512]{2,1,0:T(2,128)(2,1)S(1)} %bitcast.81, bf16[]{:T(256)} %broadcast.119), dimensions={1}, to_apply=%bitcast.78.reduce_sub_computation | reduce | bytes 983042
  172.5 1.0 reshape.198
  173.5 5.5 %all-to-all-start.1 = ((bf16[8,2,15360]{2,1,0:T(2,128)(2,1)}), bf16[8,2,15360]{2,1,0:T(2,128)(2,1)S(1)}, u32[]{:S(2)}, u32[]{:S(2)}) async-start(bf16[8,2,15360]{2,1,0:T(2,128)(2,1)} %reshape.198), calls=%async_computation.1 | async-start | bytes 983040 | tf_op jit(solution)/shard_map/all_to_all | solution.py:118
  179.0 0.2 copy.71
  179.3 1.7 fusion.43
  181.1 1.7 fusion.25
  182.8 6.3 %all_gather.25 = bf16[192,1024]{1,0:T(8,128)(2,1)S(1)} all-gather(bf16[192,256]{1,0:T(8,128)(2,1)S(1)} %fusion.25), channel_id=1, replica_groups=mesh['sp'=8,'tp'=4] {'tp'}, dimensions={1}, use_global_device_ids=true | all-gather | bytes 491520 | tf_op jit(solution)/shard_map/all_gather | solution.py:109
  189.1 4.2 %all-to-all-done.1 = bf16[8,2,15360]{2,1,0:T(2,128)(2,1)S(1)} async-done(((bf16[8,2,15360]{2,1,0:T(2,128)(2,1)}), bf16[8,2,15360]{2,1,0:T(2,128)(2,1)S(1)}, u32[]{:S(2)}, u32[]{:S(2)}) %all-to-all-start.1) | async-done | bytes 491552 | tf_op jit(solution)/shard_map/all_to_all | solution.py:118
  193.3 0.4 reshape.199
  193.9 2.1 gather_fusion.1
  195.9 0.2 gather.15
  196.1 1.6 multiply_reduce_fusion
  197.7 2.0 fusion.24
  (51 shorter events, 1.2 us)
Async XLA Ops:
  6.5 160.3 %copy-start = (bf16[1,1024,512]{2,1,0:T(8,128)(2,1)S(1)}, bf16[1,1024,512]{2,1,0:T(8,128)(2,1)}, u32[]{:S(2)}) copy-start(bf16[1,1024,512]{2,1,0:T(8,128)(2,1)} %param.28) | copy-start | bytes 3145732
  6.5 147.0 %all-gather.2.cloned.1.call-start = ((), (), s32[]{:S(2)}) async-start(), calls=%async_computation.2 | async-start | bytes 2457600 | tf_op jit(solution)/shard_map/all_gather | solution.py:103
  50.5 4.5 %copy-start.2 = (bf16[192,256]{1,0:T(8,128)(2,1)S(1)}, bf16[192,256]{1,0:T(8,128)(2,1)}, u32[]{:S(2)}) copy-start(bf16[192,256]{1,0:T(8,128)(2,1)} %param.19) | copy-start | bytes 294916
  87.4 4.1 %copy-start.5 = (f32[4]{0:T(128)S(1)}, f32[4]{0:T(128)}, u32[]{:S(2)}) copy-start(f32[4]{0:T(128)} %param.20) | copy-start | bytes 52
  87.4 4.2 %copy-start.7 = (f32[64]{0:T(128)S(1)}, f32[64]{0:T(128)}, u32[]{:S(2)}) copy-start(f32[64]{0:T(128)} %param.21) | copy-start | bytes 772
  87.4 11.6 %copy-start.9 = (bf16[1024,512]{1,0:T(8,128)(2,1)S(1)}, bf16[1024,512]{1,0:T(8,128)(2,1)}, u32[]{:S(2)}) copy-start(bf16[1024,512]{1,0:T(8,128)(2,1)} %param.22) | copy-start | bytes 3145732
  87.4 11.5 %copy-start.11 = (bf16[192,512]{1,0:T(8,128)(2,1)S(1)}, bf16[192,512]{1,0:T(8,128)(2,1)}, u32[]{:S(2)}) copy-start(bf16[192,512]{1,0:T(8,128)(2,1)} %param.16) | copy-start | bytes 589828
  91.4 17.7 %copy-start.4 = (f32[2048]{0:T(1024)S(1)}, f32[2048]{0:T(1024)}, u32[]{:S(2)}) copy-start(f32[2048]{0:T(1024)} %param.23) | copy-start | bytes 24580
  133.3 22.9 %copy-start.10 = (bf16[1,256,2048]{2,1,0:T(8,128)(2,1)S(1)}, bf16[1,256,2048]{2,1,0:T(8,128)(2,1)}, u32[]{:S(2)}) copy-start(bf16[1,256,2048]{2,1,0:T(8,128)(2,1)} %param.27) | copy-start | bytes 3145732
  153.6 2.7 %copy-start.8 = (bf16[1,480,2048]{2,1,0:T(8,128)(2,1)S(1)}, bf16[1,480,2048]{2,1,0:T(8,128)(2,1)}, u32[]{:S(2)}) copy-start(bf16[1,480,2048]{2,1,0:T(8,128)(2,1)} %all-gather.2.cloned.1.call-done) | copy-start | bytes 5898244
  157.0 22.0 %copy-start.3 = (s32[192,2]{0,1:T(2,128)S(1)}, s32[192,2]{0,1:T(2,128)}, u32[]{:S(2)}) copy-start(s32[192,2]{0,1:T(2,128)} %param.24) | copy-start | bytes 4612
  157.0 22.2 %copy-start.6 = (f32[192,2]{0,1:T(2,128)S(1)}, f32[192,2]{0,1:T(2,128)}, u32[]{:S(2)}) copy-start(f32[192,2]{0,1:T(2,128)} %param.25) | copy-start | bytes 4612
  173.5 19.8 %all-to-all-start.1 = ((bf16[8,2,15360]{2,1,0:T(2,128)(2,1)}), bf16[8,2,15360]{2,1,0:T(2,128)(2,1)S(1)}, u32[]{:S(2)}, u32[]{:S(2)}) async-start(bf16[8,2,15360]{2,1,0:T(2,128)(2,1)} %reshape.198), calls=%async_computation.1 | async-start | bytes 983040 | tf_op jit(solution)/shard_map/all_to_all | solution.py:118
  193.9 3.9 %copy-start.1 = (bf16[1024,512]{1,0:T(8,128)(2,1)S(1)}, bf16[1024,512]{1,0:T(8,128)(2,1)}, u32[]{:S(2)}) copy-start(bf16[1024,512]{1,0:T(8,128)(2,1)} %param.31) | copy-start | bytes 3145732
Sparse Core Ops, SparseCore 0:
  133.3 20.2 all-gather.1
where the time goes:
time: 207 us
  blocking collectives  119 us (57%)
  waiting for transfers between devices  24.4 us (12%)
  matrix products  16.5 us (8%)
  local copies, waits for them, and re-layouts  15.1 us (7%)
  between operations  13.8 us (7%)
  other arithmetic  12.6 us (6%)
  starting transfers between devices  5.51 us (3%)
    all_gather x1, blocking collectives, body(): key_piece = lax.all_gather(key_rows, 'sp', axis=0, tiled=True)  34.1 us
    all_gather x1, blocking collectives, body(): value_piece = lax.all_gather(value_rows, 'sp', axis=0, tiled=True)  32.1 us
    all_to_all x1, blocking collectives, body(): lax.all_to_all(outgoing, 'sp', split_axis=0, concat_axis=1, tiled=True)  20.3 us
    all_gather x1, waiting for transfers between devices, body(): pieces = lax.all_gather(arrived, 'tp', axis=2, tiled=True)  20.1 us
    all_gather x1, blocking collectives, body(): lax.all_gather(expert_flat, 'tp', axis=1, tiled=True)  9.84 us
    all_gather x1, blocking collectives, body(): full_rows = lax.all_gather(hidden_state, 'tp', axis=1, tiled=True)  8.9 us
    all_gather x1, blocking collectives, body(): lax.all_gather(head_out, 'tp', axis=1, tiled=True)  7.21 us
    all_gather x1, blocking collectives, body(): lax.all_gather(shared_hidden, 'tp', axis=1, tiled=True)  6.29 us
  transfers between devices with their start and end apart: 2, of which 2 were waited for; matrix products, arithmetic and copies ran while one was open for 2% of the time, Pallas kernels for 0%

commit v1 on v0

--- a/solution.py
+++ b/solution.py
@@ -1,10 +1,15 @@
+import functools
+
 import jax
 import jax.numpy as jnp
 from jax import lax
+from jax.experimental import pallas as pl
+from jax.experimental.pallas import tpu as pltpu
 from jax.sharding import PartitionSpec as P
 
 epsilon = 1e-06
 masked_score = -1e30
+MESH = pl.DeviceIdType.MESH
 
 
 def rms_scale(values, gain_vec):
@@ -128,6 +133,596 @@
     return (hidden_state.astype(jnp.float32) + shared_add + routed).astype(jnp.bfloat16)
 
 
+def lane_iota(rows):
+    return lax.broadcasted_iota(jnp.int32, (rows, 128), 1)
+
+
+def roll_half(values):
+    return pltpu.roll(values, 64, 1)
+
+
+def contract_last(a, b):
+    return lax.dot_general(a, b, (((1,), (1,)), ((), ())), preferred_element_type=jnp.float32)
+
+
+def layer_kernel(
+    n_sp,
+    n_tp,
+    q_in,
+    k_in,
+    v_in,
+    res_in,
+    map_w,
+    head_g,
+    norm_g,
+    slot_row,
+    slot_col,
+    route_w,
+    out_proj,
+    exp_gate,
+    exp_up,
+    exp_down,
+    sh_gate,
+    sh_up,
+    sh_down,
+    out_ref,
+    w_out,
+    w_gate,
+    w_up,
+    w_down,
+    w_sgate,
+    w_sup,
+    w_sdown,
+    kv_out,
+    q_out,
+    kv_buf,
+    q_buf,
+    o_out,
+    ho_buf,
+    hid_buf,
+    disp_out,
+    arr_buf,
+    sh_buf,
+    eh_buf,
+    res_out,
+    ret_buf,
+    w_sem,
+    a_send,
+    kv_recv,
+    q_recv,
+    o_send,
+    o_recv,
+    d_send,
+    d_recv,
+    r_send,
+    r_recv,
+    g_send,
+    g_recv,
+):
+    me_s = lax.axis_index("sp")
+    me_t = lax.axis_index("tp")
+    sib = me_t + 1 - 2 * lax.rem(me_t, 2)
+    peers = n_tp // 2 - 1
+    rows = res_in.shape[0]
+    col_dev = res_in.shape[1]
+    half = rows // 2
+    quarter = rows // 4
+    cap = arr_buf.shape[2]
+    half_dim = 32
+    groups = eh_buf.shape[1]
+    per_group = n_sp // groups
+    bf16 = jnp.bfloat16
+    f32 = jnp.float32
+
+    loads = []
+    for i, (src, dst) in enumerate(
+        (
+            (out_proj, w_out),
+            (sh_gate, w_sgate),
+            (sh_up, w_sup),
+            (exp_gate.at[0], w_gate),
+            (exp_up.at[0], w_up),
+            (exp_down.at[0], w_down),
+            (sh_down, w_sdown),
+        )
+    ):
+        copy = pltpu.make_async_copy(src, dst, w_sem.at[i])
+        copy.start()
+        loads.append(copy)
+
+    barrier = pltpu.get_barrier_semaphore()
+    for d in range(1, n_sp):
+        pl.semaphore_signal(
+            barrier, inc=1, device_id={"sp": lax.rem(me_s + d, n_sp)}, device_id_type=MESH
+        )
+    for d in range(1, n_tp):
+        pl.semaphore_signal(
+            barrier, inc=1, device_id={"tp": lax.rem(me_t + d, n_tp)}, device_id_type=MESH
+        )
+
+    sends = []
+
+    def send(src, dst, ssem, rsem, device):
+        copy = pltpu.make_async_remote_copy(
+            src_ref=src,
+            dst_ref=dst,
+            send_sem=ssem,
+            recv_sem=rsem,
+            device_id=device,
+            device_id_type=MESH,
+        )
+        copy.start()
+        return copy
+
+    def wait_recv(ref, ssem, rsem, device):
+        pltpu.make_async_remote_copy(
+            src_ref=ref,
+            dst_ref=ref,
+            send_sem=ssem,
+            recv_sem=rsem,
+            device_id=device,
+            device_id_type=MESH,
+        ).wait_recv()
+
+    n_gs = 1 + 2 * peers
+
+    def gather_start(piece, get):
+        for k in range(1, peers + 1):
+            other = lax.rem(me_t + 2 * k, n_tp)
+            sends.append(
+                send(
+                    get(me_t),
+                    get(me_t),
+                    g_send.at[piece * n_gs + k],
+                    g_recv.at[piece * n_tp + me_t],
+                    {"tp": other},
+                )
+            )
+        sends.append(
+            send(
+                get(me_t),
+                get(me_t),
+                g_send.at[piece * n_gs],
+                g_recv.at[piece * n_tp + me_t],
+                {"tp": sib},
+            )
+        )
+
+    def gather_relay(piece, get):
+        for k in range(1, peers + 1):
+            other = lax.rem(me_t + 2 * k, n_tp)
+            wait_recv(
+                get(other), g_send.at[piece * n_gs], g_recv.at[piece * n_tp + other], {"tp": sib}
+            )
+            sends.append(
+                send(
+                    get(other),
+                    get(other),
+                    g_send.at[piece * n_gs + peers + k],
+                    g_recv.at[piece * n_tp + other],
+                    {"tp": sib},
+                )
+            )
+
+    def gather_finish(piece, get):
+        for k in range(peers + 1):
+            other = lax.rem(sib + 2 * k, n_tp)
+            wait_recv(
+                get(other), g_send.at[piece * n_gs], g_recv.at[piece * n_tp + other], {"tp": sib}
+            )
+
+    low_rows = lane_iota(rows) < 64
+    low_quarter = lane_iota(quarter) < 64
+    for j in range(n_sp // 4):
+        pair = slice(j * 128, (j + 1) * 128)
+        keys = k_in[:, pair].astype(f32)
+        vals = v_in[:, pair].astype(f32)
+        kv_out[2 * j] = jnp.where(low_rows, keys, roll_half(vals)).astype(bf16)
+        kv_out[2 * j + 1] = jnp.where(low_rows, roll_half(keys), vals).astype(bf16)
+        for p in range(2):
+            first = q_in[p * half : p * half + quarter, pair].astype(f32)
+            second = q_in[p * half + quarter : (p + 1) * half, pair].astype(f32)
+            q_out[4 * j + p] = jnp.where(low_quarter, first, roll_half(second)).astype(bf16)
+            q_out[4 * j + 2 + p] = jnp.where(low_quarter, roll_half(first), second).astype(bf16)
+
+    pl.semaphore_wait(barrier, n_sp + n_tp - 2)
+
+    for d in range(1, n_sp):
+        dst = lax.rem(me_s + d, n_sp)
+        sends.append(
+            send(
+                kv_out.at[dst // 2],
+                kv_buf.at[me_s],
+                a_send.at[2 * d],
+                kv_recv.at[me_s],
+                {"sp": dst},
+            )
+        )
+        sends.append(
+            send(
+                q_out.at[dst], q_buf.at[me_s], a_send.at[2 * d + 1], q_recv.at[me_s], {"sp": dst}
+            )
+        )
+    kv_buf[me_s] = kv_out[me_s // 2]
+    q_buf[me_s] = q_out[me_s]
+
+    parity = lax.rem(me_s, 2)
+    lane_q = lane_iota(quarter)
+    scale = half_dim ** (-0.5)
+    row_in = lax.broadcasted_iota(jnp.int32, (half, rows), 0) + parity * half
+    visible_half = lax.broadcasted_iota(jnp.int32, (half, rows), 1) <= row_in
+    visible = jnp.concatenate([visible_half.astype(f32)] * 2, axis=0) > 0.5
+    high_lanes = lane_iota(half) >= 64
+    zero_q = jnp.zeros((quarter, 128), f32)
+    for s in range(n_sp):
+
+        @pl.when(me_s != s)
+        def _():
+            wait_recv(kv_buf.at[s], a_send.at[0], kv_recv.at[s], {"sp": s})
+            wait_recv(q_buf.at[s], a_send.at[1], q_recv.at[s], {"sp": s})
+
+        packed = q_buf[s].astype(f32)
+        rolled = roll_half(packed)
+        first_map = lane_q < 32
+        second_map = (lane_q >= 32) & (lane_q < 64)
+        queries = jnp.concatenate(
+            [
+                jnp.where(first_map, packed, zero_q),
+                jnp.where(first_map, rolled, zero_q),
+                jnp.where(second_map, packed, zero_q),
+                jnp.where(second_map, rolled, zero_q),
+            ],
+            axis=0,
+        ).astype(bf16)
+        diag = contract_last(queries, kv_buf[s]) * scale
+        diag = jnp.where(visible, diag, masked_score)
+        row_max = jnp.max(diag, axis=1, keepdims=True)
+        if s:
+            before = kv_buf[0:s].reshape(s * rows, 128)
+            early = contract_last(queries, before) * scale
+            row_max = jnp.maximum(row_max, jnp.max(early, axis=1, keepdims=True))
+        expo = jnp.where(visible, jnp.exp(diag - row_max), 0.0)
+        total = jnp.sum(expo, axis=1, keepdims=True)
+        acc = jnp.dot(expo.astype(bf16), kv_buf[s], preferred_element_type=f32)
+        if s:
+            expo_early = jnp.exp(early - row_max)
+            total = total + jnp.sum(expo_early, axis=1, keepdims=True)
+            acc = acc + jnp.dot(expo_early.astype(bf16), before, preferred_element_type=f32)
+        summed = acc / total
+        diff = summed[0:half] - map_w[...] * summed[half:rows]
+        diff = jnp.where(high_lanes, diff, 0.0)
+        squares = jnp.sum(diff * diff, axis=1, keepdims=True) * (1.0 / 64.0)
+        head = diff * lax.rsqrt(squares + epsilon) * head_g[...]
+        o_out[s] = (roll_half(head[0:quarter]) + head[quarter:half]).astype(bf16)
+
+        @pl.when(me_s != s)
+        def _():
+            send(
+                o_out.at[s],
+                ho_buf.at[me_t, me_s],
+                o_send.at[s],
+                o_recv.at[me_s],
+                {"sp": s},
+            )
+
+        @pl.when(me_s == s)
+        def _():
+            ho_buf[me_t, s] = o_out[s]
+
+    for s in range(n_sp):
+
+        @pl.when(me_s != s)
+        def _():
+            wait_recv(ho_buf.at[me_t, s], o_send.at[s], o_recv.at[s], {"sp": s})
+
+    def get_ho(t):
+        return ho_buf.at[t]
+
+    gather_start(0, get_ho)
+
+    slots = n_sp * cap
+    slot_iota = lax.broadcasted_iota(jnp.int32, (slots, rows), 0)
+    chosen = (slot_iota == slot_row[0:1, :]) | (slot_iota == slot_row[1:2, :])
+    spread = jnp.where(chosen, 1.0, 0.0).astype(bf16)
+    gather_relay(0, get_ho)
+    gather_finish(0, get_ho)
+
+    blocks = []
+    for p in range(2):
+        for u in range(2):
+            parts = []
+            for t in range(n_tp):
+                for j in range(n_sp // 4):
+                    even = ho_buf[t, 4 * j + p].astype(f32)
+                    odd = ho_buf[t, 4 * j + 2 + p].astype(f32)
+                    if u == 0:
+                        part = jnp.where(low_quarter, even, roll_half(odd))
+                    else:
+                        part = jnp.where(low_quarter, roll_half(even), odd)
+                    parts.append(part.astype(bf16))
+            blocks.append(jnp.concatenate(parts, axis=1))
+    heads = jnp.concatenate(blocks, axis=0)
+    loads[0].wait()
+    attn = jnp.dot(heads, w_out[...], preferred_element_type=f32)
+    hidden = (res_in[...].astype(f32) + attn).astype(bf16)
+    hid_buf[me_t] = hidden
+
+    def get_hid(t):
+        return hid_buf.at[t]
+
+    gather_start(1, get_hid)
+
+    outgoing = jnp.dot(spread, hidden, preferred_element_type=f32).astype(bf16)
+    disp_out[...] = outgoing.reshape(n_sp, cap, col_dev)
+    for d in range(1, n_sp):
+        sends.append(
+            send(
+                disp_out.at[d],
+                arr_buf.at[me_t, d],
+                d_send.at[d],
+                d_recv.at[d],
+                {"sp": lax.rem(me_s + d, n_sp)},
+            )
+        )
+    arr_buf[me_t, 0] = disp_out[0]
+
+    def get_arr(d):
+        return lambda t: arr_buf.at[t, d]
+
+    gather_start(2, get_arr(0))
+    gather_relay(1, get_hid)
+
+    def normalise(pieces):
+        full = [piece.astype(f32) for piece in pieces]
+        squares = sum(jnp.sum(piece * piece, axis=1, keepdims=True) for piece in full)
+        factor = lax.rsqrt(squares * (1.0 / (n_tp * col_dev)) + epsilon)
+        return jnp.concatenate(
+            [
+                (piece * factor * norm_g[:, t * col_dev : (t + 1) * col_dev]).astype(bf16)
+                for t, piece in enumerate(full)
+            ],
+            axis=1,
+        )
+
+    def gated(normed, gate, up):
+        gate_part = contract_last(normed, gate[...])
+        up_part = contract_last(normed, up[...])
+        return (gate_part / (1.0 + jnp.exp(-gate_part)) * up_part).astype(bf16)
+
+    def arrive(d):
+        wait_recv(
+            arr_buf.at[me_t, d], d_send.at[d], d_recv.at[d], {"sp": lax.rem(me_s + d, n_sp)}
+        )
+        gather_start(2 + d, get_arr(d))
+        gather_relay(1 + d, get_arr(d - 1))
+
+    def get_sh(t):
+        return sh_buf.at[t]
+
+    def get_eh(g):
+        return lambda t: eh_buf.at[t, g]
+
+    piece_sh = 2 + n_sp
+    piece_eh = 3 + n_sp
+
+    def expert_up(g):
+        ds = range(g * per_group, (g + 1) * per_group)
+        for d in ds:
+            gather_finish(2 + d, get_arr(d))
+        normed = normalise(
+            [
+                arr_buf[t, g * per_group : (g + 1) * per_group].reshape(per_group * cap, col_dev)
+                for t in range(n_tp)
+            ]
+        )
+        eh_buf[me_t, g] = gated(normed, w_gate, w_up)
+        gather_start(piece_eh + g, get_eh(g))
+
+    def expert_out(g):
+        gather_finish(piece_eh + g, get_eh(g))
+        joined = jnp.concatenate([eh_buf[t, g] for t in range(n_tp)], axis=1)
+        result = jnp.dot(joined, w_down[...], preferred_element_type=f32).astype(bf16)
+        res_out[g * per_group : (g + 1) * per_group] = result.reshape(per_group, cap, col_dev)
+        for d in range(g * per_group, (g + 1) * per_group):
+            if d == 0:
+                ret_buf[0] = res_out[0]
+            else:
+                sends.append(
+                    send(
+                        res_out.at[d],
+                        ret_buf.at[d],
+                        r_send.at[d],
+                        r_recv.at[d],
+                        {"sp": lax.rem(me_s + n_sp - d, n_sp)},
+                    )
+                )
+
+    arrive(1)
+    arrive(2)
+    gather_finish(1, get_hid)
+    loads[1].wait()
+    loads[2].wait()
+    normed_own = normalise([hid_buf[t] for t in range(n_tp)])
+    sh_buf[me_t] = gated(normed_own, w_sgate, w_sup)
+    gather_start(piece_sh, get_sh)
+    for i in range(3, 7):
+        loads[i].wait()
+    done = 0
+    for d in range(3, n_sp):
+        arrive(d)
+        if (d - 1) % per_group == per_group - 1 and d > per_group - 1:
+            expert_up(done)
+            done += 1
+    gather_relay(1 + n_sp, get_arr(n_sp - 1))
+    gather_relay(piece_sh, get_sh)
+    for g in range(done):
+        gather_relay(piece_eh + g, get_eh(g))
+    for g in range(groups):
+        if g == done:
+            expert_up(g)
+            done += 1
+        if g + 1 == done and g == groups - 1:
+            gather_relay(piece_eh + g, get_eh(g))
+        if g + 1 == groups - 1 and done == groups - 1:
+            expert_up(g + 1)
+            done += 1
+        expert_out(g)
+
+    gather_finish(piece_sh, get_sh)
+    shared_all = jnp.concatenate([sh_buf[t] for t in range(n_tp)], axis=1)
+    result = hid_buf[me_t].astype(f32) + jnp.dot(
+        shared_all, w_sdown[...], preferred_element_type=f32
+    )
+    col_iota = lax.broadcasted_iota(jnp.int32, (rows, slots), 1)
+    picks = [
+        jnp.where(col_iota == slot_col[:, c : c + 1], 1.0, 0.0).astype(bf16) for c in range(2)
+    ]
+    for d in range(1, n_sp):
+        wait_recv(ret_buf.at[d], r_send.at[d], r_recv.at[d], {"sp": lax.rem(me_s + d, n_sp)})
+    returned = ret_buf[...].reshape(slots, col_dev)
+    for c in range(2):
+        picked = jnp.dot(picks[c], returned, preferred_element_type=f32)
+        result = result + route_w[:, c : c + 1] * picked
+    out_ref[...] = result.astype(out_ref.dtype)
+
+    for copy in sends:
+        copy.wait_send()
+    for s in range(n_sp):
+
+        @pl.when(me_s != s)
+        def _():
+            pltpu.make_async_remote_copy(
+                src_ref=o_out.at[s],
+                dst_ref=ho_buf.at[me_t, me_s],
+                send_sem=o_send.at[s],
+                recv_sem=o_recv.at[me_s],
+                device_id={"sp": s},
+                device_id_type=MESH,
+            ).wait_send()
+
+
+def fused_body(
+    residual_in,
+    query_rows,
+    key_rows,
+    value_rows,
+    map_weight,
+    head_gain,
+    out_proj,
+    norm_gain,
+    route_ids,
+    route_weights,
+    expert_gate,
+    expert_up,
+    expert_down,
+    shared_gate,
+    shared_up,
+    shared_down,
+):
+    n_sp = lax.axis_size("sp")
+    n_tp = lax.axis_size("tp")
+    rows, col_dev = residual_in.shape
+    topk = route_ids.shape[1]
+    capacity = 5 * rows * topk // (4 * n_sp)
+    cap = (capacity + 15) // 16 * 16
+    hid_units = shared_gate.shape[0]
+    width = shared_gate.shape[1]
+    me_s = lax.axis_index("sp")
+    flat = route_ids.reshape(-1)
+    order = jnp.arange(flat.shape[0], dtype=jnp.int32)
+    same = (flat[:, None] == flat[None, :]) & (order[None, :] < order[:, None])
+    position = jnp.sum(same.astype(jnp.int32), axis=1)
+    place = lax.rem(flat - me_s + n_sp, n_sp)
+    slot_col = (place * cap + position).reshape(rows, topk)
+    slot_row = slot_col.T
+    map_vec = jnp.broadcast_to(
+        lax.dynamic_slice_in_dim(map_weight, me_s // 2, 1)[None, :], (1, 128)
+    )
+    gain_vec = jnp.concatenate([jnp.zeros((64,), jnp.float32), head_gain])[None, :]
+    bf16 = jnp.bfloat16
+    groups = 2
+    pieces = 3 + n_sp + groups
+    n_gs = 1 + 2 * (n_tp // 2 - 1)
+    dma = pltpu.SemaphoreType.DMA
+    vmem = pl.BlockSpec(memory_space=pltpu.VMEM)
+    hbm = pl.BlockSpec(memory_space=pl.ANY)
+    return pl.pallas_call(
+        functools.partial(layer_kernel, n_sp, n_tp),
+        out_shape=jax.ShapeDtypeStruct((rows, col_dev), bf16),
+        in_specs=[vmem] * 10 + [hbm] * 7,
+        out_specs=vmem,
+        scratch_shapes=[
+            pltpu.VMEM(out_proj.shape, bf16),
+            pltpu.VMEM(expert_gate.shape[1:], bf16),
+            pltpu.VMEM(expert_up.shape[1:], bf16),
+            pltpu.VMEM(expert_down.shape[1:], bf16),
+            pltpu.VMEM(shared_gate.shape, bf16),
+            pltpu.VMEM(shared_up.shape, bf16),
+            pltpu.VMEM(shared_down.shape, bf16),
+            pltpu.VMEM((n_sp // 2, rows, 128), bf16),
+            pltpu.VMEM((n_sp, rows // 4, 128), bf16),
+            pltpu.VMEM((n_sp, rows, 128), bf16),
+            pltpu.VMEM((n_sp, rows // 4, 128), bf16),
+            pltpu.VMEM((n_sp, rows // 4, 128), bf16),
+            pltpu.VMEM((n_tp, n_sp, rows // 4, 128), bf16),
+            pltpu.VMEM((n_tp, rows, col_dev), bf16),
+            pltpu.VMEM((n_sp, cap, col_dev), bf16),
+            pltpu.VMEM((n_tp, n_sp, cap, col_dev), bf16),
+            pltpu.VMEM((n_tp, rows, hid_units), bf16),
+            pltpu.VMEM((n_tp, groups, n_sp // groups * cap, hid_units), bf16),
+            pltpu.VMEM((n_sp, cap, col_dev), bf16),
+            pltpu.VMEM((n_sp, cap, col_dev), bf16),
+            dma((7,)),
+            dma((2 * n_sp,)),
+            dma((n_sp,)),
+            dma((n_sp,)),
+            dma((n_sp,)),
+            dma((n_sp,)),
+            dma((n_sp,)),
+            dma((n_sp,)),
+            dma((n_sp,)),
+            dma((n_sp,)),
+            dma((pieces * n_gs,)),
+            dma((pieces * n_tp,)),
+        ],
+        compiler_params=pltpu.CompilerParams(collective_id=0, has_side_effects=True),
+    )(
+        query_rows,
+        key_rows,
+        value_rows,
+        residual_in,
+        map_vec,
+        gain_vec,
+        norm_gain[None, :],
+        slot_row,
+        slot_col,
+        route_weights,
+        out_proj,
+        expert_gate,
+        expert_up,
+        expert_down,
+        shared_gate,
+        shared_up,
+        shared_down,
+    )
+
+
+def layer(*args):
+    residual_in, map_weight, head_gain, route_ids = args[0], args[4], args[5], args[8]
+    fits = (
+        2 * map_weight.shape[0] == lax.axis_size("sp")
+        and map_weight.shape[0] % 2 == 0
+        and head_gain.shape[0] == 64
+        and route_ids.shape[1] == 2
+        and args[10].shape[0] == 1
+        and residual_in.shape[0] % 64 == 0
+        and residual_in.shape[1] % 128 == 0
+        and args[13].shape[0] % 128 == 0
+        and lax.axis_size("tp") % 2 == 0
+    )
+    return (fused_body if fits else body)(*args)
+
+
 def solution(mesh):
     in_specs = (
         P("sp", "tp"),
@@ -148,4 +743,4 @@
         P(None, "tp"),
     )
     out_specs = P("sp", "tp")
-    return jax.shard_map(body, mesh=mesh, in_specs=in_specs, out_specs=out_specs, check_vma=False)
+    return jax.shard_map(layer, mesh=mesh, in_specs=in_specs, out_specs=out_specs, check_vma=False)

time: 207 us -> 88.9 us (0.43)
  blocking collectives: 119 us -> 0 us
  Pallas kernels: 0 us -> 81 us
  waiting for transfers between devices: 24.4 us -> 0 us
  matrix products: 16.5 us -> 0 us
  between operations: 13.8 us -> 0.07 us
  other arithmetic: 12.6 us -> 0.28 us
  local copies, waits for them, and re-layouts: 15.1 us -> 7.37 us
  starting transfers between devices: 5.51 us -> 0 us
    all_gather x6 -> x0, blocking collectives: 98.4 us -> none  [the longest x1 34.1 us: body(): key_piece = lax.all_gather(key_rows, 'sp', axis=0, tiled=True)]
    pallas_call x0 -> x1, Pallas kernels: none -> 81 us  [fused_body(): pl.pallas_call(functools.partial(layer_kernel, n_sp, n_tp), out_shape=jax...]
    all_to_all x1 -> x0, blocking collectives: 20.3 us -> none  [body(): lax.all_to_all(outgoing, 'sp', split_axis=0, concat_axis=1, tiled=True)]
    all_gather x1 -> x0, waiting for transfers between devices: 20.1 us -> none  [body(): pieces = lax.all_gather(arrived, 'tp', axis=2, tiled=True)]
    dot_general x9 -> x0, matrix products: 16.5 us -> none  [the longest x1 4.03 us: body(): jnp.einsum('mhqk,khd->mhqd', expo.astype(jnp.bfloat16), value_heads, pref...]
    reduce_sum x5 -> x1, other arithmetic: 6.5 us -> 0.24 us  [fused_body(): position = jnp.sum(same.astype(jnp.int32), axis=1)]
    all_to_all x1 -> x0, starting transfers between devices: 5.51 us -> none  [body(): lax.all_to_all(expert_add.astype(jnp.bfloat16), 'sp', split_axis=1, conca...]
    gather x4 -> x0, local copies, waits for them, and re-layouts: 4.44 us -> none  [the longest x2 2.22 us: body(): jnp.take(padded, slot_token, axis=0).reshape(experts_all, capacity, col_dev)]
  transfers between devices with their start and end apart: 2 -> 0, of which waited for: 2 -> 0; matrix products, arithmetic and copies ran while one was open for 2% -> 0% of each run, Pallas kernels for 0% -> 0%
where the time goes in v1:
time: 88.9 us; the launch traced here: 88.7 us
  Pallas kernels  81 us (91%)
  local copies, waits for them, and re-layouts  7.37 us (8%)
    pallas_call x1, Pallas kernels, fused_body(): pl.pallas_call(functools.partial(layer_kernel, n_sp, n_tp), out_shape=jax...  81 us
    unnamed x13, local copies, waits for them, and re-layouts  3.72 us

profile of v1, /device:TPU:0, one launch (start us, length us, event | category | flops | bytes accessed | tf_op | source)
XLA Modules:
  0.0 88.7 jit_solution(9591461028135441118)
XLA Ops:
  0.0 0.0 copy-start.3
  0.0 0.7 copy-done.3
  0.7 0.6 dynamic_slice.3
  1.2 0.0 copy-start.4
  1.2 0.0 copy-start.1
  1.2 1.2 %broadcast_in_dim.18.map_w = f32[1,128]{1,0:T(1,128)} broadcast(f32[]{:T(128)} %bitcast), dimensions={} | broadcast | bytes 516 | tf_op jit(solution)/shard_map/broadcast_in_dim | solution.py:638
  2.5 0.0 copy-done.4
  2.5 0.6 pad_bitcast_fusion.head_g
  3.1 0.0 copy-done.1
  3.1 0.2 copy.49
  3.3 0.0 copy-start.2
  3.3 0.1 copy.46
  3.4 0.6 copy-done.2
  4.0 0.8 copy.52.route_w
  4.7 0.1 copy.50
  4.9 0.1 eq.15
  5.0 0.2 convert_reduce_fusion
  5.2 0.1 reduce_sum.12
  5.4 0.0 copy-start
  5.5 0.6 copy.51.slot_row
  6.1 0.0 copy-done
  6.1 81.0 %shard_map.154 = bf16[192,512]{1,0:T(8,128)(2,1)} custom-call(bf16[192,256]{1,0:T(8,128)(2,1)} %q_in.1, bf16[192,256]{1,0:T(8,128)(2,1)} %k_in.1, bf16[192,256]{1,0:T(8,128)(2,1)} %v_in.1, bf16[192,512]{1,0:T(8,128)(2,1)} %res_in.1, f32[1,128]{1,0:T(1,128)} %broadcast_in_dim.18.map_w, f32[1,128]{1,0:T(1,128)} %pad_bitcast_fusion.head_g, f32[1,2048]{1,0:T(1,128)} %bitcast.6, ...), custom_call_target="tpu_custom_call" | custom-call | tf_op jit(solution)/shard_map/pallas_call | solution.py:649
  87.1 1.6 %copy.54 = bf16[192,512]{1,0:T(8,128)(2,1)} copy(bf16[192,512]{1,0:T(8,128)(2,1)} %shard_map.154) | data formatting | bytes 393216
  (2 shorter events, 0.0 us)
Async XLA Ops:
  0.0 0.7 copy-start.3
  1.2 1.2 %copy-start.4 = (f32[64]{0:T(128)S(1)}, f32[64]{0:T(128)}, u32[]{:S(2)}) copy-start(f32[64]{0:T(128)} %param.21) | copy-start | bytes 772
  1.2 1.9 %copy-start.1 = (s32[192,2]{0,1:T(2,128)S(1)}, s32[192,2]{0,1:T(2,128)}, u32[]{:S(2)}) copy-start(s32[192,2]{0,1:T(2,128)} %param.24) | copy-start | bytes 4612
  3.3 0.7 copy-start.2
  5.4 0.7 copy-start

commit v2 on v1

--- a/solution.py
+++ b/solution.py
@@ -155,8 +155,7 @@
     map_w,
     head_g,
     norm_g,
-    slot_row,
-    slot_col,
+    ids_in,
     route_w,
     out_proj,
     exp_gate,
@@ -186,6 +185,9 @@
     eh_buf,
     res_out,
     ret_buf,
+    spread_buf,
+    pick_buf,
+    weight_buf,
     w_sem,
     a_send,
     kv_recv,
@@ -214,6 +216,14 @@
     bf16 = jnp.bfloat16
     f32 = jnp.float32
 
+    def across(k):
+        other = me_s
+        for b in range(n_sp.bit_length() - 1):
+            if k >> b & 1:
+                bit = lax.rem(me_s // (1 << b), 2)
+                other = other + (1 << b) * (1 - 2 * bit)
+        return other
+
     loads = []
     for i, (src, dst) in enumerate(
         (
@@ -328,7 +338,7 @@
     pl.semaphore_wait(barrier, n_sp + n_tp - 2)
 
     for d in range(1, n_sp):
-        dst = lax.rem(me_s + d, n_sp)
+        dst = across(d)
         sends.append(
             send(
                 kv_out.at[dst // 2],
@@ -345,6 +355,41 @@
         )
     kv_buf[me_s] = kv_out[me_s // 2]
     q_buf[me_s] = q_out[me_s]
+
+    eye = lax.broadcasted_iota(jnp.int32, (rows, rows), 0)
+    eye_lane = lax.broadcasted_iota(jnp.int32, (rows, rows), 1)
+    same = eye == eye_lane
+    before_col = eye_lane < eye
+    before_row = eye < eye_lane
+
+    def as_column(row):
+        return jnp.sum(jnp.where(same, row, 0.0), axis=1, keepdims=True)
+
+    ids_row = [jnp.bitwise_xor(ids_in[c : c + 1, :], me_s).astype(f32) for c in range(2)]
+    ids_col = [as_column(row) for row in ids_row]
+    weight_col = [as_column(route_w[c : c + 1, :]) for c in range(2)]
+    slot_row = []
+    slot_col = []
+    for c in range(2):
+        hit = (ids_row[0] == ids_col[c]) | (ids_row[1] == ids_col[c])
+        count = jnp.sum(jnp.where(hit & before_col, 1.0, 0.0), axis=1, keepdims=True)
+        slot_col.append(ids_col[c] * cap + count)
+        hit = (ids_col[0] == ids_row[c]) | (ids_col[1] == ids_row[c])
+        count = jnp.sum(jnp.where(hit & before_row, 1.0, 0.0), axis=0, keepdims=True)
+        slot_row.append(ids_row[c] * cap + count)
+    slots = n_sp * cap
+    slot_iota = lax.broadcasted_iota(jnp.int32, (slots, rows), 0).astype(f32)
+    chosen = (slot_iota == slot_row[0]) | (slot_iota == slot_row[1])
+    spread_buf[...] = jnp.where(chosen, 1.0, 0.0).astype(bf16)
+    col_iota = lax.broadcasted_iota(jnp.int32, (rows, slots), 1).astype(f32)
+    for c in range(2):
+        pick_buf[c] = jnp.where(col_iota == slot_col[c], 1.0, 0.0).astype(bf16)
+        weight_buf[c] = jnp.broadcast_to(weight_col[c], (rows, 128))
+    head_lane = lax.broadcasted_iota(jnp.int32, map_w.shape, 1)
+    map_here = jnp.sum(
+        jnp.where(head_lane == me_s // 2, map_w[...], 0.0), axis=1, keepdims=True
+    )
+    gain_here = jnp.concatenate([jnp.zeros((1, 64), f32), head_g[...]], axis=1)
 
     parity = lax.rem(me_s, 2)
     lane_q = lane_iota(quarter)
@@ -389,10 +434,10 @@
             total = total + jnp.sum(expo_early, axis=1, keepdims=True)
             acc = acc + jnp.dot(expo_early.astype(bf16), before, preferred_element_type=f32)
         summed = acc / total
-        diff = summed[0:half] - map_w[...] * summed[half:rows]
+        diff = summed[0:half] - map_here * summed[half:rows]
         diff = jnp.where(high_lanes, diff, 0.0)
         squares = jnp.sum(diff * diff, axis=1, keepdims=True) * (1.0 / 64.0)
-        head = diff * lax.rsqrt(squares + epsilon) * head_g[...]
+        head = diff * lax.rsqrt(squares + epsilon) * gain_here
         o_out[s] = (roll_half(head[0:quarter]) + head[quarter:half]).astype(bf16)
 
         @pl.when(me_s != s)
@@ -409,23 +454,25 @@
         def _():
             ho_buf[me_t, s] = o_out[s]
 
-    for s in range(n_sp):
-
-        @pl.when(me_s != s)
-        def _():
-            wait_recv(ho_buf.at[me_t, s], o_send.at[s], o_recv.at[s], {"sp": s})
-
-    def get_ho(t):
-        return ho_buf.at[t]
-
-    gather_start(0, get_ho)
-
-    slots = n_sp * cap
-    slot_iota = lax.broadcasted_iota(jnp.int32, (slots, rows), 0)
-    chosen = (slot_iota == slot_row[0:1, :]) | (slot_iota == slot_row[1:2, :])
-    spread = jnp.where(chosen, 1.0, 0.0).astype(bf16)
-    gather_relay(0, get_ho)
-    gather_finish(0, get_ho)
+    split = n_sp // 2
+    near = me_s // split * split
+
+    def get_near(t):
+        return ho_buf.at[t, pl.ds(near, split)]
+
+    def get_far(t):
+        return ho_buf.at[t, pl.ds(split - near, split)]
+
+    for d in range(1, n_sp):
+        if d == split:
+            gather_start(0, get_near)
+        other = across(d)
+        wait_recv(ho_buf.at[me_t, other], o_send.at[d], o_recv.at[other], {"sp": other})
+    gather_start(3 + n_sp + groups, get_far)
+    for piece, get in ((0, get_near), (3 + n_sp + groups, get_far)):
+        gather_relay(piece, get)
+    for piece, get in ((0, get_near), (3 + n_sp + groups, get_far)):
+        gather_finish(piece, get)
 
     blocks = []
     for p in range(2):
@@ -452,8 +499,8 @@
 
     gather_start(1, get_hid)
 
-    outgoing = jnp.dot(spread, hidden, preferred_element_type=f32).astype(bf16)
-    disp_out[...] = outgoing.reshape(n_sp, cap, col_dev)
+    outgoing = jnp.dot(spread_buf[cap:slots], hidden, preferred_element_type=f32).astype(bf16)
+    disp_out[1:n_sp] = outgoing.reshape(n_sp - 1, cap, col_dev)
     for d in range(1, n_sp):
         sends.append(
             send(
@@ -461,16 +508,12 @@
                 arr_buf.at[me_t, d],
                 d_send.at[d],
                 d_recv.at[d],
-                {"sp": lax.rem(me_s + d, n_sp)},
-            )
-        )
-    arr_buf[me_t, 0] = disp_out[0]
+                {"sp": across(d)},
+            )
+        )
 
     def get_arr(d):
         return lambda t: arr_buf.at[t, d]
-
-    gather_start(2, get_arr(0))
-    gather_relay(1, get_hid)
 
     def normalise(pieces):
         full = [piece.astype(f32) for piece in pieces]
@@ -490,11 +533,11 @@
         return (gate_part / (1.0 + jnp.exp(-gate_part)) * up_part).astype(bf16)
 
     def arrive(d):
-        wait_recv(
-            arr_buf.at[me_t, d], d_send.at[d], d_recv.at[d], {"sp": lax.rem(me_s + d, n_sp)}
-        )
+        wait_recv(arr_buf.at[me_t, d], d_send.at[d], d_recv.at[d], {"sp": across(d)})
         gather_start(2 + d, get_arr(d))
-        gather_relay(1 + d, get_arr(d - 1))
+
+    def relay(d):
+        gather_relay(2 + d, get_arr(d))
 
     def get_sh(t):
         return sh_buf.at[t]
@@ -508,7 +551,8 @@
     def expert_up(g):
         ds = range(g * per_group, (g + 1) * per_group)
         for d in ds:
-            gather_finish(2 + d, get_arr(d))
+            if d:
+                gather_finish(2 + d, get_arr(d))
         normed = normalise(
             [
                 arr_buf[t, g * per_group : (g + 1) * per_group].reshape(per_group * cap, col_dev)
@@ -533,56 +577,60 @@
                         ret_buf.at[d],
                         r_send.at[d],
                         r_recv.at[d],
-                        {"sp": lax.rem(me_s + n_sp - d, n_sp)},
+                        {"sp": across(d)},
                     )
                 )
 
+    def relay_eh(g):
+        gather_relay(piece_eh + g, get_eh(g))
+
     arrive(1)
     arrive(2)
+    gather_relay(1, get_hid)
+    arrive(3)
+    relay(1)
+    relay(2)
     gather_finish(1, get_hid)
     loads[1].wait()
     loads[2].wait()
     normed_own = normalise([hid_buf[t] for t in range(n_tp)])
     sh_buf[me_t] = gated(normed_own, w_sgate, w_sup)
-    gather_start(piece_sh, get_sh)
+    for t in range(n_tp):
+        arr_buf[t, 0] = jnp.dot(
+            spread_buf[0:cap], hid_buf[t], preferred_element_type=f32
+        ).astype(bf16)
     for i in range(3, 7):
         loads[i].wait()
-    done = 0
-    for d in range(3, n_sp):
+    for d in range(4, n_sp):
         arrive(d)
-        if (d - 1) % per_group == per_group - 1 and d > per_group - 1:
-            expert_up(done)
-            done += 1
-    gather_relay(1 + n_sp, get_arr(n_sp - 1))
+        relay(d - 1)
+        if d % 2:
+            expert_up((d - 5) // 2)
+    expert_up(groups - 2)
+    for g in range(groups - 2):
+        relay_eh(g)
+    for g in range(groups - 2):
+        expert_out(g)
+    relay(n_sp - 1)
+    relay_eh(groups - 2)
+    expert_up(groups - 1)
+    expert_out(groups - 2)
+    gather_start(piece_sh, get_sh)
+    relay_eh(groups - 1)
     gather_relay(piece_sh, get_sh)
-    for g in range(done):
-        gather_relay(piece_eh + g, get_eh(g))
-    for g in range(groups):
-        if g == done:
-            expert_up(g)
-            done += 1
-        if g + 1 == done and g == groups - 1:
-            gather_relay(piece_eh + g, get_eh(g))
-        if g + 1 == groups - 1 and done == groups - 1:
-            expert_up(g + 1)
-            done += 1
-        expert_out(g)
+    expert_out(groups - 1)
 
     gather_finish(piece_sh, get_sh)
     shared_all = jnp.concatenate([sh_buf[t] for t in range(n_tp)], axis=1)
     result = hid_buf[me_t].astype(f32) + jnp.dot(
         shared_all, w_sdown[...], preferred_element_type=f32
     )
-    col_iota = lax.broadcasted_iota(jnp.int32, (rows, slots), 1)
-    picks = [
-        jnp.where(col_iota == slot_col[:, c : c + 1], 1.0, 0.0).astype(bf16) for c in range(2)
-    ]
     for d in range(1, n_sp):
-        wait_recv(ret_buf.at[d], r_send.at[d], r_recv.at[d], {"sp": lax.rem(me_s + d, n_sp)})
+        wait_recv(ret_buf.at[d], r_send.at[d], r_recv.at[d], {"sp": across(d)})
     returned = ret_buf[...].reshape(slots, col_dev)
     for c in range(2):
-        picked = jnp.dot(picks[c], returned, preferred_element_type=f32)
-        result = result + route_w[:, c : c + 1] * picked
+        picked = jnp.dot(pick_buf[c], returned, preferred_element_type=f32)
+        result = result + weight_buf[c][:, 0:1] * picked
     out_ref[...] = result.astype(out_ref.dtype)
 
     for copy in sends:
@@ -626,22 +674,9 @@
     capacity = 5 * rows * topk // (4 * n_sp)
     cap = (capacity + 15) // 16 * 16
     hid_units = shared_gate.shape[0]
-    width = shared_gate.shape[1]
-    me_s = lax.axis_index("sp")
-    flat = route_ids.reshape(-1)
-    order = jnp.arange(flat.shape[0], dtype=jnp.int32)
-    same = (flat[:, None] == flat[None, :]) & (order[None, :] < order[:, None])
-    position = jnp.sum(same.astype(jnp.int32), axis=1)
-    place = lax.rem(flat - me_s + n_sp, n_sp)
-    slot_col = (place * cap + position).reshape(rows, topk)
-    slot_row = slot_col.T
-    map_vec = jnp.broadcast_to(
-        lax.dynamic_slice_in_dim(map_weight, me_s // 2, 1)[None, :], (1, 128)
-    )
-    gain_vec = jnp.concatenate([jnp.zeros((64,), jnp.float32), head_gain])[None, :]
     bf16 = jnp.bfloat16
-    groups = 2
-    pieces = 3 + n_sp + groups
+    groups = n_sp // 2
+    pieces = 4 + n_sp + groups
     n_gs = 1 + 2 * (n_tp // 2 - 1)
     dma = pltpu.SemaphoreType.DMA
     vmem = pl.BlockSpec(memory_space=pltpu.VMEM)
@@ -649,7 +684,7 @@
     return pl.pallas_call(
         functools.partial(layer_kernel, n_sp, n_tp),
         out_shape=jax.ShapeDtypeStruct((rows, col_dev), bf16),
-        in_specs=[vmem] * 10 + [hbm] * 7,
+        in_specs=[vmem] * 9 + [hbm] * 7,
         out_specs=vmem,
         scratch_shapes=[
             pltpu.VMEM(out_proj.shape, bf16),
@@ -672,6 +707,9 @@
             pltpu.VMEM((n_tp, groups, n_sp // groups * cap, hid_units), bf16),
             pltpu.VMEM((n_sp, cap, col_dev), bf16),
             pltpu.VMEM((n_sp, cap, col_dev), bf16),
+            pltpu.VMEM((n_sp * cap, rows), bf16),
+            pltpu.VMEM((2, rows, n_sp * cap), bf16),
+            pltpu.VMEM((2, rows, 128), jnp.float32),
             dma((7,)),
             dma((2 * n_sp,)),
             dma((n_sp,)),
@@ -691,12 +729,11 @@
         key_rows,
         value_rows,
         residual_in,
-        map_vec,
-        gain_vec,
+        map_weight[None, :],
+        head_gain[None, :],
         norm_gain[None, :],
-        slot_row,
-        slot_col,
-        route_weights,
+        route_ids.T,
+        route_weights.T,
         out_proj,
         expert_gate,
         expert_up,
@@ -710,7 +747,7 @@
 def layer(*args):
     residual_in, map_weight, head_gain, route_ids = args[0], args[4], args[5], args[8]
     fits = (
-        2 * map_weight.shape[0] == lax.axis_size("sp")
+        2 * map_weight.shape[0] == lax.axis_size("sp") == 8
         and map_weight.shape[0] % 2 == 0
         and head_gain.shape[0] == 64
         and route_ids.shape[1] == 2

time: 88.9 us -> 76.3 us (0.86)
  Pallas kernels: 81 us -> 74.5 us
  local copies, waits for them, and re-layouts: 7.37 us -> 1.62 us
    pallas_call x1, Pallas kernels: 81 us -> 74.5 us  [fused_body(): pl.pallas_call(functools.partial(layer_kernel, n_sp, n_tp), out_shape=jax...]
    unnamed x13 -> x1, local copies, waits for them, and re-layouts: 3.72 us -> 1.62 us
    broadcast_in_dim x2 -> x0, local copies, waits for them, and re-layouts: 1.86 us -> none  [the longest x1 1.22 us: fused_body(): jnp.broadcast_to(lax.dynamic_slice_in_dim(map_weight, me_s // 2, 1)[None,...]
where the time goes in v2:
time: 76.3 us; the launch traced here: 76.2 us
  Pallas kernels  74.5 us (98%)
  local copies, waits for them, and re-layouts  1.62 us (2%)
    pallas_call x1, Pallas kernels, fused_body(): pl.pallas_call(functools.partial(layer_kernel, n_sp, n_tp), out_shape=jax...  74.5 us
    unnamed x1, local copies, waits for them, and re-layouts  1.62 us

profile of v2, /device:TPU:0, one launch (start us, length us, event | category | flops | bytes accessed | tf_op | source)
XLA Modules:
  0.0 76.2 jit_solution(18440298406235572451)
XLA Ops:
  0.0 74.5 %shard_map.154 = bf16[192,512]{1,0:T(8,128)(2,1)} custom-call(bf16[192,256]{1,0:T(8,128)(2,1)} %q_in.1, bf16[192,256]{1,0:T(8,128)(2,1)} %k_in.1, bf16[192,256]{1,0:T(8,128)(2,1)} %v_in.1, bf16[192,512]{1,0:T(8,128)(2,1)} %res_in.1, f32[1,4]{1,0:T(1,128)} %bitcast.8, f32[1,64]{1,0:T(1,128)} %bitcast.9, f32[1,2048]{1,0:T(1,128)} %bitcast.5, ...), custom_call_target="tpu_custom_call" | custom-call | tf_op jit(solution)/shard_map/pallas_call | solution.py:684
  74.5 1.6 %copy.18 = bf16[192,512]{1,0:T(8,128)(2,1)} copy(bf16[192,512]{1,0:T(8,128)(2,1)} %shard_map.154) | data formatting | bytes 393216

commit v3 on v2

--- a/solution.py
+++ b/solution.py
@@ -560,7 +560,6 @@
             ]
         )
         eh_buf[me_t, g] = gated(normed, w_gate, w_up)
-        gather_start(piece_eh + g, get_eh(g))
 
     def expert_out(g):
         gather_finish(piece_eh + g, get_eh(g))
@@ -584,41 +583,56 @@
     def relay_eh(g):
         gather_relay(piece_eh + g, get_eh(g))
 
+    def start_eh(g):
+        gather_start(piece_eh + g, get_eh(g))
+
+    def relay_eh(g):
+        gather_relay(piece_eh + g, get_eh(g))
+
     arrive(1)
     arrive(2)
     gather_relay(1, get_hid)
     arrive(3)
     relay(1)
     relay(2)
+    arrive(4)
     gather_finish(1, get_hid)
     loads[1].wait()
     loads[2].wait()
     normed_own = normalise([hid_buf[t] for t in range(n_tp)])
     sh_buf[me_t] = gated(normed_own, w_sgate, w_sup)
+    relay(3)
+    arrive(5)
+    relay(4)
     for t in range(n_tp):
         arr_buf[t, 0] = jnp.dot(
             spread_buf[0:cap], hid_buf[t], preferred_element_type=f32
         ).astype(bf16)
     for i in range(3, 7):
         loads[i].wait()
-    for d in range(4, n_sp):
-        arrive(d)
-        relay(d - 1)
-        if d % 2:
-            expert_up((d - 5) // 2)
-    expert_up(groups - 2)
-    for g in range(groups - 2):
-        relay_eh(g)
-    for g in range(groups - 2):
-        expert_out(g)
-    relay(n_sp - 1)
-    relay_eh(groups - 2)
-    expert_up(groups - 1)
-    expert_out(groups - 2)
+    expert_up(0)
+    arrive(6)
+    relay(5)
+    expert_up(2)
+    start_eh(2)
+    arrive(7)
+    relay(6)
+    expert_up(1)
+    relay_eh(2)
+    relay(7)
+    expert_out(2)
+    expert_up(3)
+    start_eh(3)
+    start_eh(1)
+    start_eh(0)
     gather_start(piece_sh, get_sh)
-    relay_eh(groups - 1)
+    relay_eh(3)
+    expert_out(3)
+    relay_eh(1)
+    relay_eh(0)
     gather_relay(piece_sh, get_sh)
-    expert_out(groups - 1)
+    expert_out(1)
+    expert_out(0)
 
     gather_finish(piece_sh, get_sh)
     shared_all = jnp.concatenate([sh_buf[t] for t in range(n_tp)], axis=1)

time: 76.3 us -> 74.2 us (0.972)
  Pallas kernels: 74.5 us -> 72.5 us
    pallas_call x1, Pallas kernels: 74.5 us -> 72.5 us  [fused_body(): pl.pallas_call(functools.partial(layer_kernel, n_sp, n_tp), out_shape=jax...]
where the time goes in v3:
time: 74.2 us; the launch traced here: 74.1 us
  Pallas kernels  72.5 us (98%)
  local copies, waits for them, and re-layouts  1.62 us (2%)
    pallas_call x1, Pallas kernels, fused_body(): pl.pallas_call(functools.partial(layer_kernel, n_sp, n_tp), out_shape=jax...  72.5 us
    unnamed x1, local copies, waits for them, and re-layouts  1.62 us

profile of v3, /device:TPU:0, one launch (start us, length us, event | category | flops | bytes accessed | tf_op | source)
XLA Modules:
  0.0 74.1 jit_solution(14858275700178827611)
XLA Ops:
  0.0 72.5 %shard_map.154 = bf16[192,512]{1,0:T(8,128)(2,1)} custom-call(bf16[192,256]{1,0:T(8,128)(2,1)} %q_in.1, bf16[192,256]{1,0:T(8,128)(2,1)} %k_in.1, bf16[192,256]{1,0:T(8,128)(2,1)} %v_in.1, bf16[192,512]{1,0:T(8,128)(2,1)} %res_in.1, f32[1,4]{1,0:T(1,128)} %bitcast.8, f32[1,64]{1,0:T(1,128)} %bitcast.9, f32[1,2048]{1,0:T(1,128)} %bitcast.5, ...), custom_call_target="tpu_custom_call" | custom-call | tf_op jit(solution)/shard_map/pallas_call | solution.py:698
  72.5 1.6 %copy.18 = bf16[192,512]{1,0:T(8,128)(2,1)} copy(bf16[192,512]{1,0:T(8,128)(2,1)} %shard_map.154) | data formatting | bytes 393216

commit v4 on v3

--- a/solution.py
+++ b/solution.py
@@ -337,7 +337,7 @@
 
     pl.semaphore_wait(barrier, n_sp + n_tp - 2)
 
-    for d in range(1, n_sp):
+    for d in (6, 7, 4, 5, 2, 3, 1):
         dst = across(d)
         sends.append(
             send(
@@ -399,60 +399,68 @@
     visible = jnp.concatenate([visible_half.astype(f32)] * 2, axis=0) > 0.5
     high_lanes = lane_iota(half) >= 64
     zero_q = jnp.zeros((quarter, 128), f32)
-    for s in range(n_sp):
-
-        @pl.when(me_s != s)
-        def _():
-            wait_recv(kv_buf.at[s], a_send.at[0], kv_recv.at[s], {"sp": s})
-            wait_recv(q_buf.at[s], a_send.at[1], q_recv.at[s], {"sp": s})
-
-        packed = q_buf[s].astype(f32)
-        rolled = roll_half(packed)
-        first_map = lane_q < 32
-        second_map = (lane_q >= 32) & (lane_q < 64)
-        queries = jnp.concatenate(
-            [
-                jnp.where(first_map, packed, zero_q),
-                jnp.where(first_map, rolled, zero_q),
-                jnp.where(second_map, packed, zero_q),
-                jnp.where(second_map, rolled, zero_q),
-            ],
-            axis=0,
-        ).astype(bf16)
-        diag = contract_last(queries, kv_buf[s]) * scale
-        diag = jnp.where(visible, diag, masked_score)
-        row_max = jnp.max(diag, axis=1, keepdims=True)
-        if s:
-            before = kv_buf[0:s].reshape(s * rows, 128)
-            early = contract_last(queries, before) * scale
-            row_max = jnp.maximum(row_max, jnp.max(early, axis=1, keepdims=True))
-        expo = jnp.where(visible, jnp.exp(diag - row_max), 0.0)
-        total = jnp.sum(expo, axis=1, keepdims=True)
-        acc = jnp.dot(expo.astype(bf16), kv_buf[s], preferred_element_type=f32)
-        if s:
-            expo_early = jnp.exp(early - row_max)
-            total = total + jnp.sum(expo_early, axis=1, keepdims=True)
-            acc = acc + jnp.dot(expo_early.astype(bf16), before, preferred_element_type=f32)
-        summed = acc / total
-        diff = summed[0:half] - map_here * summed[half:rows]
-        diff = jnp.where(high_lanes, diff, 0.0)
-        squares = jnp.sum(diff * diff, axis=1, keepdims=True) * (1.0 / 64.0)
-        head = diff * lax.rsqrt(squares + epsilon) * gain_here
-        o_out[s] = (roll_half(head[0:quarter]) + head[quarter:half]).astype(bf16)
-
-        @pl.when(me_s != s)
-        def _():
-            send(
-                o_out.at[s],
-                ho_buf.at[me_t, me_s],
-                o_send.at[s],
-                o_recv.at[me_s],
-                {"sp": s},
-            )
-
-        @pl.when(me_s == s)
-        def _():
-            ho_buf[me_t, s] = o_out[s]
+    first_map = lane_q < 32
+    second_map = (lane_q >= 32) & (lane_q < 64)
+    batch = n_sp // 2
+    for start in range(0, n_sp, batch):
+        steps = range(start, start + batch)
+        for s in steps:
+
+            @pl.when(me_s != s)
+            def _():
+                wait_recv(kv_buf.at[s], a_send.at[0], kv_recv.at[s], {"sp": s})
+                wait_recv(q_buf.at[s], a_send.at[1], q_recv.at[s], {"sp": s})
+
+        queries = {}
+        for s in steps:
+            packed = q_buf[s].astype(f32)
+            rolled = roll_half(packed)
+            queries[s] = jnp.concatenate(
+                [
+                    jnp.where(first_map, packed, zero_q),
+                    jnp.where(first_map, rolled, zero_q),
+                    jnp.where(second_map, packed, zero_q),
+                    jnp.where(second_map, rolled, zero_q),
+                ],
+                axis=0,
+            ).astype(bf16)
+        keys = {s: kv_buf[0 : s + 1].reshape((s + 1) * rows, 128) for s in steps}
+        scores = {}
+        for s in steps:
+            raw = contract_last(queries[s], keys[s]) * scale
+            diag = jnp.where(visible, raw[:, s * rows :], masked_score)
+            scores[s] = jnp.concatenate([raw[:, : s * rows], diag], axis=1) if s else diag
+        row_max = {s: jnp.max(scores[s], axis=1, keepdims=True) for s in steps}
+        expo = {s: jnp.exp(scores[s] - row_max[s]) for s in steps}
+        total = {s: jnp.sum(expo[s], axis=1, keepdims=True) for s in steps}
+        acc = {
+            s: jnp.dot(expo[s].astype(bf16), keys[s], preferred_element_type=f32) for s in steps
+        }
+        diff = {}
+        for s in steps:
+            summed = acc[s] / total[s]
+            raw = summed[0:half] - map_here * summed[half:rows]
+            diff[s] = jnp.where(high_lanes, raw, 0.0)
+        for s in steps:
+            squares = jnp.sum(diff[s] * diff[s], axis=1, keepdims=True) * (1.0 / 64.0)
+            head = diff[s] * lax.rsqrt(squares + epsilon) * gain_here
+            o_out[s] = (roll_half(head[0:quarter]) + head[quarter:half]).astype(bf16)
+
+        for s in steps:
+
+            @pl.when(me_s != s)
+            def _():
+                send(
+                    o_out.at[s],
+                    ho_buf.at[me_t, me_s],
+                    o_send.at[s],
+                    o_recv.at[me_s],
+                    {"sp": s},
+                )
+
+            @pl.when(me_s == s)
+            def _():
+                ho_buf[me_t, s] = o_out[s]
 
     split = n_sp // 2
     near = me_s // split * split

time: 74.2 us -> 72.2 us (0.973)
  Pallas kernels: 72.5 us -> 70.4 us
    pallas_call x1, Pallas kernels: 72.5 us -> 70.4 us  [fused_body(): pl.pallas_call(functools.partial(layer_kernel, n_sp, n_tp), out_shape=jax...]
where the time goes in v4:
time: 72.2 us; the launch traced here: 72 us
  Pallas kernels  70.4 us (98%)
  local copies, waits for them, and re-layouts  1.62 us (2%)
    pallas_call x1, Pallas kernels, fused_body(): pl.pallas_call(functools.partial(layer_kernel, n_sp, n_tp), out_shape=jax...  70.4 us
    unnamed x1, local copies, waits for them, and re-layouts  1.62 us

profile of v4, /device:TPU:0, one launch (start us, length us, event | category | flops | bytes accessed | tf_op | source)
XLA Modules:
  0.0 72.0 jit_solution(1146839097535165125)
XLA Ops:
  0.0 70.4 %shard_map.154 = bf16[192,512]{1,0:T(8,128)(2,1)} custom-call(bf16[192,256]{1,0:T(8,128)(2,1)} %q_in.1, bf16[192,256]{1,0:T(8,128)(2,1)} %k_in.1, bf16[192,256]{1,0:T(8,128)(2,1)} %v_in.1, bf16[192,512]{1,0:T(8,128)(2,1)} %res_in.1, f32[1,4]{1,0:T(1,128)} %bitcast.8, f32[1,64]{1,0:T(1,128)} %bitcast.9, f32[1,2048]{1,0:T(1,128)} %bitcast.5, ...), custom_call_target="tpu_custom_call" | custom-call | tf_op jit(solution)/shard_map/pallas_call | solution.py:706
  70.4 1.6 %copy.18 = bf16[192,512]{1,0:T(8,128)(2,1)} copy(bf16[192,512]{1,0:T(8,128)(2,1)} %shard_map.154) | data formatting | bytes 393216

commit v5 on v4

--- a/solution.py
+++ b/solution.py
@@ -623,24 +623,24 @@
     relay(5)
     expert_up(2)
     start_eh(2)
+    expert_up(1)
     arrive(7)
+    start_eh(1)
+    start_eh(0)
     relay(6)
-    expert_up(1)
     relay_eh(2)
     relay(7)
     expert_out(2)
     expert_up(3)
     start_eh(3)
-    start_eh(1)
-    start_eh(0)
     gather_start(piece_sh, get_sh)
+    relay_eh(1)
+    relay_eh(0)
+    expert_out(1)
+    expert_out(0)
     relay_eh(3)
     expert_out(3)
-    relay_eh(1)
-    relay_eh(0)
     gather_relay(piece_sh, get_sh)
-    expert_out(1)
-    expert_out(0)
 
     gather_finish(piece_sh, get_sh)
     shared_all = jnp.concatenate([sh_buf[t] for t in range(n_tp)], axis=1)

time: 72.2 us -> 69.8 us (0.967)
  Pallas kernels: 70.4 us -> 67.6 us
    pallas_call x1, Pallas kernels: 70.4 us -> 67.6 us  [fused_body(): pl.pallas_call(functools.partial(layer_kernel, n_sp, n_tp), out_shape=jax...]
where the time goes in v5:
time: 69.8 us; the launch traced here: 69.3 us
  Pallas kernels  67.6 us (97%)
  local copies, waits for them, and re-layouts  1.62 us (2%)
    pallas_call x1, Pallas kernels, fused_body(): pl.pallas_call(functools.partial(layer_kernel, n_sp, n_tp), out_shape=jax...  67.6 us
    unnamed x1, local copies, waits for them, and re-layouts  1.62 us

profile of v5, /device:TPU:0, one launch (start us, length us, event | category | flops | bytes accessed | tf_op | source)
XLA Modules:
  0.0 69.3 jit_solution(146876330381917372)
XLA Ops:
  0.0 67.6 %shard_map.154 = bf16[192,512]{1,0:T(8,128)(2,1)} custom-call(bf16[192,256]{1,0:T(8,128)(2,1)} %q_in.1, bf16[192,256]{1,0:T(8,128)(2,1)} %k_in.1, bf16[192,256]{1,0:T(8,128)(2,1)} %v_in.1, bf16[192,512]{1,0:T(8,128)(2,1)} %res_in.1, f32[1,4]{1,0:T(1,128)} %bitcast.8, f32[1,64]{1,0:T(1,128)} %bitcast.9, f32[1,2048]{1,0:T(1,128)} %bitcast.5, ...), custom_call_target="tpu_custom_call" | custom-call | tf_op jit(solution)/shard_map/pallas_call | solution.py:706
  67.6 1.6 %copy.18 = bf16[192,512]{1,0:T(8,128)(2,1)} copy(bf16[192,512]{1,0:T(8,128)(2,1)} %shard_map.154) | data formatting | bytes 393216
